TPU v7x, 32 devices: a whole 2x2x4 slice. The times are simulated.
32 devices in a mesh: ep: 8 (over z, x), tp: 4 (over y, core).
Axes of the slice: x: 2, y: 2, z: 4, core: 2. Of those that a mesh axis runs over, the one named last changes fastest.
Arguments:
- query_in: bfloat16 [4096, 2048], P('ep', 'tp'), may hold values from -6 to 6
- key_in: bfloat16 [4096, 2048], P('ep', 'tp'), may hold values from -6 to 6
- value_in: bfloat16 [4096, 2048], P('ep', 'tp'), may hold values from -6 to 6
- gate_in: bfloat16 [4096, 2048], P('ep', 'tp'), may hold values from -6 to 6
- decay_rate: float32 [16], P('tp'), may hold values from 0 to 0.04
- head_gain: float32 [2048], P('tp'), may hold values from 0.1 to 1.9
- output_weight: bfloat16 [2048, 2048], P('tp'), may hold values from -0.125 to 0.125
- token_rows: bfloat16 [1536, 2048], P('ep'), may hold values from -100 to 100
- token_gain: float32 [2048], replicated, may hold values from 0.1 to 1.9
- route_ids: int32 [1536, 2], P('ep'), may hold values from 0 to 7, all different within a row; in each aligned block of 192 rows (0 to 191, 192 to 383, ...) at most 96 rows name the same one
- route_weights: float32 [1536, 2], P('ep'), may hold values from 0.25 to 2.5
- expert_gate: bfloat16 [8, 2048, 4096], P('ep', None, 'tp'), may hold values from -0.125 to 0.125
- expert_up: bfloat16 [8, 2048, 4096], P('ep', None, 'tp'), may hold values from -0.125 to 0.125
- expert_down: bfloat16 [8, 4096, 2048], P('ep', None, 'tp'), may hold values from -0.09375 to 0.09375
Outputs:
- retained_out: bfloat16 [4096, 2048], P(('ep', 'tp'))
- expert_out: bfloat16 [1536, 2048], P('ep', 'tp')
Inputs may be any that keep to these rules, and one draw needn't show every extreme that they name: `route_ids`: each row names 2 different experts. In each aligned block of 192 rows (the rows of one index of ep) no expert is named by more than 96 rows, a bound that some block reaches.
All inputs are finite; a program needn't handle non-finite values.
Results may differ from a plain program's by a relative error of at most 0.019.
Values may be sent and summed in bfloat16 or wider, within the bound.
A program may use at most 64 MiB of HBM per device.

v0:
```python
import functools

import jax
import jax.numpy as jnp
import numpy as np
from jax import lax
from jax.experimental import pallas as pl
from jax.experimental.pallas import tpu as pltpu
from jax.sharding import PartitionSpec as P

epsilon = 1e-06
rope_base = 10000.0
NF, NM, FAN, EARLY = 8, 4, 2, 4
F32 = jnp.float32
BF16 = jnp.bfloat16
MESH = pl.DeviceIdType.MESH


def dot(a, b):
    return jnp.dot(a, b, preferred_element_type=F32)


def iota(shape, dim):
    return lax.broadcasted_iota(jnp.int32, shape, dim)


def silu(v):
    return v / (1.0 + jnp.exp(-v))


def kernel(
    size,
    tok, tgain, ids_t, rweights_t, decay, hgain, freq, turn_sign,
    query_h, key_h, value_h, gate_h, ow_h, wg_h, wu_h, wd_h,
    ret_out, exp_out,
    query, key, value, gate, ow, wg, wu, wd,
    obuf, xbuf, hbuf, sbuf, rbuf, w_hi, w_lo, cos_t, sin_t,
    rq, rk, local, state, st_send, st_recv, mixed, part, rs1, rs2_send, rs2_recv,
    load_sem, d_send, d_recv, xy_send, xy_recv, xc_send, xc_recv,
    hy_send, hy_recv, hc_send, hc_recv, b_send, b_recv, st_ssem, st_rsem,
    r1_send, r1_recv, r2_send, r2_recv,
):
    ep, tp, cap, fan, rounds, nf, nm = (
        size["ep"], size["tp"], size["cap"], size["fan"], size["rounds"], size["nf"], size["nm"]
    )
    ys = tp // 2
    e, t = lax.axis_index("ep"), lax.axis_index("tp")
    y, c = t // 2, lax.rem(t, 2)
    mate = (e, y * 2 + 1 - c)
    heads = decay.shape[0]
    tokens, model = tok.shape
    cw = model // tp
    block_len = query.shape[0]
    dk = query.shape[1] // heads

    def over_ep(offset):
        return (lax.rem(e + offset, ep), t)

    def y_at(offset):
        return lax.rem(y + offset, ys)

    def over_y(offset):
        return (e, y_at(offset) * 2 + c)

    def remote(src, dst, ssem, rsem, device):
        return pltpu.make_async_remote_copy(
            src_ref=src, dst_ref=dst, send_sem=ssem, recv_sem=rsem,
            device_id=device, device_id_type=MESH,
        )

    sent = []

    def send(src, dst, ssem, rsem, device):
        copy = remote(src, dst, ssem, rsem, device)
        copy.start()
        sent.append(copy)

    def arrived(dst, ssem, rsem, device):
        remote(dst, dst, ssem, rsem, device).wait_recv()

    loads = [
        pltpu.make_async_copy(a, b, load_sem.at[i])
        for i, (a, b) in enumerate(
            ((query_h, query), (key_h, key), (value_h, value), (gate_h, gate),
             (wg_h, wg), (wu_h, wu), (ow_h, ow), (wd_h, wd))
        )
    ]
    for copy in loads:
        copy.start()

    barrier = pltpu.get_barrier_semaphore()
    friends = [over_ep(i) for i in range(1, ep)] + [over_y(i) for i in range(1, ys)] + [mate]
    for friend in friends:
        pl.semaphore_signal(barrier, inc=1, device_id=friend, device_id_type=MESH)

    def relative(v):
        return jnp.where(v < e, v - e + ep, v - e)

    rel_t = relative(ids_t[...])
    rows = max(ep, 16)
    named0_t = iota((rows, tokens), 0) == rel_t[0:1, :]
    named1_t = iota((rows, tokens), 0) == rel_t[1:2, :]
    named_t = jnp.where(named0_t | named1_t, 1.0, 0.0)
    after = jnp.where(iota((tokens, tokens), 0) < iota((tokens, tokens), 1), 1.0, 0.0)
    rank_t = dot(named_t.astype(BF16), after.astype(BF16))
    pos0_t = rel_t[0:1, :] * cap + jnp.sum(
        jnp.where(named0_t, rank_t, 0.0), 0, keepdims=True).astype(jnp.int32)
    pos1_t = rel_t[1:2, :] * cap + jnp.sum(
        jnp.where(named1_t, rank_t, 0.0), 0, keepdims=True).astype(jnp.int32)

    rows_float = tok[...].astype(F32)
    scale = lax.rsqrt(jnp.mean(rows_float * rows_float, -1, keepdims=True) + epsilon)
    own = pl.ds(pl.multiple_of(t * cw, cw), cw)
    normed = (tok[:, own].astype(F32) * scale * tgain[:, own]).astype(BF16)
    row_id = iota((ep * cap, tokens), 0)
    pick = jnp.where((row_id == pos0_t) | (row_id == pos1_t), 1.0, 0.0).astype(BF16)
    obuf[...] = dot(pick, normed).astype(BF16)

    pl.semaphore_wait(barrier, len(friends))

    def block(j, n=1):
        return pl.ds(j * cap, n * cap)

    for j in range(ep - 1, 0, -1):
        back = ep - j
        send(obuf.at[block(j)], xbuf.at[t, block(back)], d_send.at[j], d_recv.at[back], over_ep(j))
    xbuf[t, block(0), :] = obuf[block(0), :]

    for copy in loads[:3]:
        copy.wait()
    within = iota((block_len, 1), 0).astype(F32)
    angles = (e * block_len + iota((block_len, dk), 0)).astype(F32) * freq[...]
    cos_t[...] = jnp.cos(angles)
    sin_t[...] = jnp.sin(angles) * turn_sign[...]

    def head_cols(h):
        return pl.ds(pl.multiple_of(h * dk, dk), dk)

    def turn(x):
        return x * cos_t[...] + pltpu.roll(x, dk // 2, 1) * sin_t[...]

    def head_state(h, carry):
        cols = head_cols(h)
        rate = decay[h]
        rq[:, cols] = turn(query[:, cols].astype(F32)).astype(BF16)
        rot_key = (turn(key[:, cols].astype(F32)) * dk ** (-0.5)).astype(BF16)
        rk[:, cols] = rot_key
        decayed = (rot_key.astype(F32) * jnp.exp(-rate * (block_len - 1.0 - within))).astype(BF16)
        now = lax.dot_general(
            decayed, value[:, cols], (((0,), (0,)), ((), ())), preferred_element_type=F32)
        st_send[0, h] = now.astype(BF16)
        return carry

    lax.fori_loop(0, heads, head_state, 0)
    for i in range(1, fan + 1):
        send(st_send.at[0], st_recv.at[i - 1], st_ssem.at[i - 1], st_rsem.at[i - 1], over_ep(i))

    diagonal = iota((tokens, tokens), 0) == iota((tokens, tokens), 1)

    def upright(row):
        return jnp.sum(jnp.where(diagonal, row, 0.0), 1, keepdims=True)

    col = iota((tokens, ep * cap), 1)
    pos0 = upright(pos0_t.astype(F32)).astype(jnp.int32)
    pos1 = upright(pos1_t.astype(F32)).astype(jnp.int32)
    weight = jnp.where(col == pos0, upright(rweights_t[0:1, :]), 0.0) + jnp.where(
        col == pos1, upright(rweights_t[1:2, :]), 0.0)
    high = weight.astype(BF16)
    w_hi[...] = high
    w_lo[...] = (weight - high.astype(F32)).astype(BF16)

    chunk = min(128, block_len)

    def head_local(h):
        cols = head_cols(h)
        rate = decay[h]
        key_grow = jnp.exp(rate * iota((1, block_len), 1).astype(F32))

        def step(i, carry):
            rws = pl.ds(pl.multiple_of(i * chunk, chunk), chunk)
            place = i * chunk + iota((chunk, 1), 0)
            scores = lax.dot_general(
                rq[rws, cols], rk[:, cols], (((1,), (1,)), ((), ())), preferred_element_type=F32)
            fade = jnp.exp(-rate * place.astype(F32)) * key_grow
            seen = iota((chunk, block_len), 1) <= place
            weights = jnp.where(seen, scores * fade, 0.0).astype(BF16)
            local[rws, cols] = dot(weights, value[:, cols])
            return carry

        lax.fori_loop(0, block_len // chunk, step, 0)

    def spread(buf, piece, rws, ysend, yrecv, csend, crecv, g):
        for a in range(1, ys):
            send(buf.at[piece, rws], buf.at[piece, rws], ysend.at[a, g], yrecv.at[a, g], over_y(a))
        send(buf.at[piece, rws], buf.at[piece, rws], csend.at[0, g], crecv.at[0, g], mate)

    def pass_on(buf, rws, ysend, yrecv, csend, crecv, g):
        for a in range(1, ys):
            piece = y_at(ys - a) * 2 + c
            arrived(buf.at[piece, rws], ysend.at[a, g], yrecv.at[a, g], over_y(a))
            send(buf.at[piece, rws], buf.at[piece, rws], csend.at[a, g], crecv.at[a, g], mate)

    def collect(buf, rws, csend, crecv, g):
        for a in range(ys):
            piece = y_at(ys - a) * 2 + 1 - c
            arrived(buf.at[piece, rws], csend.at[a, g], crecv.at[a, g], mate)

    per_f = ep // nf

    def x_block(f):
        return block(f * per_f, per_f)

    def x_arrive(f):
        for k in range(f * per_f, (f + 1) * per_f):
            if k > 0:
                arrived(xbuf.at[t, block(k)], d_send.at[k], d_recv.at[k], over_ep(k))
        spread(xbuf, t, x_block(f), xy_send, xy_recv, xc_send, xc_recv, f)

    def x_pass(f):
        pass_on(xbuf, x_block(f), xy_send, xy_recv, xc_send, xc_recv, f)

    f_per_m = nf // nm
    per_m = ep // nm
    ff = wg.shape[1]
    n_tile = min(256, ff)
    loads[4].wait()
    loads[5].wait()

    def lane(h, times):
        return jnp.exp(jnp.full((1, dk), -decay[h] * (block_len * times), F32))

    def first_state():
        for i in range(fan):
            arrived(st_recv.at[i], st_ssem.at[i], st_rsem.at[i], over_ep(i + 1))

        def one(h, carry):
            total = jnp.zeros((dk, dk), F32)
            for i in range(fan):
                took = st_recv[i, h].astype(F32) * lane(h, float(i))
                total += jnp.where(e > i, took, 0.0)
            state[h] = total
            return carry

        lax.fori_loop(0, heads, one, 0)

    def state_send(r):
        def one(h, carry):
            st_send[r + 1, h] = state[h].astype(BF16)
            return carry

        lax.fori_loop(0, heads, one, 0)
        send(st_send.at[r + 1], st_recv.at[fan + r], st_ssem.at[fan + r], st_rsem.at[fan + r],
             over_ep(fan * 2**r))

    def state_take(r):
        offset = fan * 2**r
        arrived(st_recv.at[fan + r], st_ssem.at[fan + r], st_rsem.at[fan + r], over_ep(offset))

        def one(h, carry):
            took = st_recv[fan + r, h].astype(F32) * lane(h, float(offset))
            state[h] = state[h] + jnp.where(e >= offset, took, 0.0)
            return carry

        lax.fori_loop(0, heads, one, 0)

    def h_pass(m):
        pass_on(hbuf, block(m * per_m, per_m), hy_send, hy_recv, hc_send, hc_recv, m)

    came = passed = done = 0
    for m in range(nm):
        need = (m + 1) * f_per_m
        while came < nf:
            x_arrive(came)
            came += 1
            while passed < came - 1:
                x_pass(passed)
                passed += 1
            if done < heads and done < EARLY:
                head_local(done)
                done += 1
        while passed < need:
            x_pass(passed)
            passed += 1
        for f in range(m * f_per_m, need):
            collect(xbuf, x_block(f), xc_send, xc_recv, f)
        rws = block(m * per_m, per_m)

        def tile(n, carry):
            cols = pl.ds(pl.multiple_of(n * n_tile, n_tile), n_tile)
            g = u = None
            for p in range(tp):
                x = xbuf[p, rws, :]
                ins = pl.ds(p * cw, cw)
                gp, up = dot(x, wg[ins, cols]), dot(x, wu[ins, cols])
                g, u = (gp, up) if g is None else (g + gp, u + up)
            hbuf[t, rws, cols] = (silu(g) * u).astype(BF16)
            return carry

        lax.fori_loop(0, ff // n_tile, tile, 0)
        spread(hbuf, t, rws, hy_send, hy_recv, hc_send, hc_recv, m)
        if m == 0:
            first_state()
            if rounds:
                state_send(0)
        elif m <= rounds:
            state_take(m - 1)
            if m < rounds:
                state_send(m)
    for r in range(nm - 1, rounds):
        if r > nm - 1:
            state_send(r)
        state_take(r)
    while done < heads:
        head_local(done)
        done += 1

    loads[3].wait()
    loads[6].wait()

    def finish(n, carry):
        h, i = n // (block_len // chunk), lax.rem(n, block_len // chunk)
        cols = head_cols(h)
        rws = pl.ds(pl.multiple_of(i * chunk, chunk), chunk)
        place = (i * chunk + iota((chunk, 1), 0)).astype(F32)
        held = state[h]
        high = held.astype(BF16)
        low = (held - high.astype(F32)).astype(BF16)
        q = rq[rws, cols]
        retained = local[rws, cols] + (dot(q, high) + dot(q, low)) * jnp.exp(
            -decay[h] * (place + 1.0))
        centered = retained - jnp.mean(retained, -1, keepdims=True)
        out = centered * lax.rsqrt(jnp.mean(centered * centered, -1, keepdims=True) + epsilon)
        mixed[rws, cols] = (out * hgain[:, cols] * silu(gate[rws, cols].astype(F32))).astype(BF16)
        return carry

    lax.fori_loop(0, heads * (block_len // chunk), finish, 0)
    rb = block_len // tp
    o_tile = min(512, model)

    def project(n, carry):
        cols = pl.ds(pl.multiple_of(n * o_tile, o_tile), o_tile)
        for d in range(tp):
            part[d, :, cols] = dot(mixed[pl.ds(d * rb, rb), :], ow[:, cols]).astype(BF16)
        return carry

    lax.fori_loop(0, model // o_tile, project, 0)
    for b in range(ys):
        send(part.at[b * 2 + 1 - c], rs1.at[b], r1_send.at[b], r1_recv.at[b], mate)

    def sum_over_cores():
        for b in range(ys):
            arrived(rs1.at[b], r1_send.at[b], r1_recv.at[b], mate)
        for a in range(1, ys):
            b = y_at(a)
            rs2_send[a - 1] = (part[b * 2 + c].astype(F32) + rs1[b].astype(F32)).astype(BF16)
            send(rs2_send.at[a - 1], rs2_recv.at[a - 1], r2_send.at[a - 1], r2_recv.at[a - 1],
                 over_y(a))

    d_tile = min(256, cw)
    loads[7].wait()
    for m in range(nm):
        h_pass(m)
        if m == 0:
            sum_over_cores()
        rws = block(m * per_m, per_m)
        collect(hbuf, rws, hc_send, hc_recv, m)

        def down(n, carry):
            cols = pl.ds(pl.multiple_of(n * d_tile, d_tile), d_tile)
            total = None
            for p in range(tp):
                now = dot(hbuf[p, rws, :], wd[pl.ds(p * ff, ff), cols])
                total = now if total is None else total + now
            sbuf[rws, cols] = total.astype(BF16)
            return carry

        lax.fori_loop(0, cw // d_tile, down, 0)
        for k in range(m * per_m, (m + 1) * per_m):
            if k > 0:
                back = ep - k
                send(sbuf.at[block(k)], rbuf.at[block(back)], b_send.at[k], b_recv.at[back],
                     over_ep(k))
            else:
                rbuf[block(0), :] = sbuf[block(0), :]

    total = part[t].astype(F32) + rs1[y].astype(F32)
    for a in range(1, ys):
        arrived(rs2_recv.at[a - 1], r2_send.at[a - 1], r2_recv.at[a - 1], over_y(a))
        total += rs2_recv[a - 1].astype(F32)
    ret_out[...] = total.astype(BF16)
    for k in range(1, ep):
        arrived(rbuf.at[block(k)], b_send.at[k], b_recv.at[k], over_ep(k))
    exp_out[...] = (dot(w_hi[...], rbuf[...]) + dot(w_lo[...], rbuf[...])).astype(BF16)
    for copy in sent:
        copy.wait_send()


def body(
    query_in, key_in, value_in, gate_in, decay_rate, head_gain, output_weight,
    token_rows, token_gain, route_ids, route_weights, expert_gate, expert_up, expert_down,
):
    ep, tp = lax.axis_size("ep"), lax.axis_size("tp")
    tokens, model = token_rows.shape
    top = route_ids.shape[1]
    cap = -(-(2 * tokens * top // ep) // 32) * 32
    block_len, width = query_in.shape
    heads = decay_rate.shape[0]
    dk = width // heads
    ff = expert_gate.shape[2]
    cw = expert_down.shape[2]
    ys = tp // 2
    fan = min(FAN, ep - 1)
    rounds = 0
    while fan * 2**rounds < ep - 1:
        rounds += 1
    nf, nm = NF, NM
    half = dk // 2
    freq = np.tile(
        np.float32(rope_base) ** (-np.arange(half, dtype=np.float32) * np.float32(2.0 / dk)), 2)
    turn_sign = np.where(np.arange(dk) < half, -1.0, 1.0)
    size = dict(ep=ep, tp=tp, cap=cap, fan=fan, rounds=rounds, nf=nf, nm=nm)
    slots = ep * cap
    rb = block_len // tp
    vmem = pl.BlockSpec(memory_space=pltpu.VMEM)
    smem = pl.BlockSpec(memory_space=pltpu.SMEM)
    hbm = pl.BlockSpec(memory_space=pl.ANY)
    dma = pltpu.SemaphoreType.DMA
    big = [query_in, key_in, value_in, gate_in, output_weight,
           expert_gate[0], expert_up[0], expert_down[0]]
    held = big
    return pl.pallas_call(
        functools.partial(kernel, size),
        out_shape=(
            jax.ShapeDtypeStruct((rb, model), BF16),
            jax.ShapeDtypeStruct((tokens, cw), BF16),
        ),
        in_specs=[vmem] * 4 + [smem] + [vmem] * 3 + [hbm] * 8,
        out_specs=(vmem, vmem),
        scratch_shapes=[pltpu.VMEM(a.shape, BF16) for a in held]
        + [
            pltpu.VMEM((slots, cw), BF16),
            pltpu.VMEM((tp, slots, cw), BF16),
            pltpu.VMEM((tp, slots, ff), BF16),
            pltpu.VMEM((slots, cw), BF16),
            pltpu.VMEM((slots, cw), BF16),
            pltpu.VMEM((tokens, slots), BF16),
            pltpu.VMEM((tokens, slots), BF16),
            pltpu.VMEM((block_len, dk), F32),
            pltpu.VMEM((block_len, dk), F32),
            pltpu.VMEM((block_len, width), BF16),
            pltpu.VMEM((block_len, width), BF16),
            pltpu.VMEM((block_len, width), F32),
            pltpu.VMEM((heads, dk, dk), F32),
            pltpu.VMEM((1 + rounds, heads, dk, dk), BF16),
            pltpu.VMEM((fan + rounds, heads, dk, dk), BF16),
            pltpu.VMEM((block_len, width), BF16),
            pltpu.VMEM((tp, rb, model), BF16),
            pltpu.VMEM((ys, rb, model), BF16),
            pltpu.VMEM((max(ys - 1, 1), rb, model), BF16),
            pltpu.VMEM((max(ys - 1, 1), rb, model), BF16),
            dma((8,)),
            dma((ep,)), dma((ep,)),
            dma((ys, nf)), dma((ys, nf)), dma((ys, nf)), dma((ys, nf)),
            dma((ys, nm)), dma((ys, nm)), dma((ys, nm)), dma((ys, nm)),
            dma((ep,)), dma((ep,)),
            dma((fan + rounds,)), dma((fan + rounds,)),
            dma((ys,)), dma((ys,)), dma((ys,)), dma((ys,)),
        ],
        compiler_params=pltpu.CompilerParams(
            collective_id=0, has_side_effects=True, vmem_limit_bytes=60 * 2**20
        ),
    )(
        token_rows, token_gain[None, :], route_ids.T, route_weights.T,
        decay_rate, head_gain[None, :],
        jnp.asarray(freq[None, :], F32), jnp.asarray(turn_sign[None, :], F32),
        *big,
    )


def solution(mesh):
    placed = (
        P("ep", "tp"), P("ep", "tp"), P("ep", "tp"), P("ep", "tp"),
        P("tp"), P("tp"), P("tp", None), P("ep", None), P(),
        P("ep", None), P("ep", None),
        P("ep", None, "tp"), P("ep", None, "tp"), P("ep", None, "tp"),
    )
    return jax.shard_map(
        body,
        mesh=mesh,
        in_specs=placed,
        out_specs=(P(("ep", "tp"), None), P("ep", "tp")),
        check_vma=False,
    )
```

profile of v0, /device:TPU:0, one launch (start us, length us, event | category | flops | bytes accessed | tf_op | source)
XLA Modules:
  0.0 91.2 jit_solution(17861167177107135739)
XLA Ops:
  0.6 87.1 %shard_map.167 = (bf16[128,2048]{1,0:T(8,128)(2,1)}, bf16[192,512]{1,0:T(8,128)(2,1)}) custom-call(bf16[192,2048]{1,0:T(8,128)(2,1)} %tok.1, f32[1,2048]{1,0:T(1,128)} %bitcast.10, s32[2,192]{1,0:T(2,128)} %bitcast.11, f32[2,192]{1,0:T(2,128)} %bitcast.12, f32[4]{0:T(128)} %decay.1, f32[1,512]{1,0:T(1,128)} %bitcast.13, f32[1,128]{1,0:T(1,128)} %constant.4.clone.freq, ...), custom_call_target="tpu_custom_call" | custom-call | tf_op jit(solution)/shard_map/pallas_call | solution.py:431
  87.7 1.9 %copy.20 = bf16[128,2048]{1,0:T(8,128)(2,1)} copy(bf16[128,2048]{1,0:T(8,128)(2,1)} %get-tuple-element.4) | data formatting | bytes 1048576
  89.6 1.6 %copy.21 = bf16[192,512]{1,0:T(8,128)(2,1)} copy(bf16[192,512]{1,0:T(8,128)(2,1)} %get-tuple-element.5) | data formatting | bytes 393216
where the time goes:
time: 92.3 us; the launch traced here: 91.2 us
  Pallas kernels  87.1 us (94%)
  local copies, waits for them, and re-layouts  3.5 us (4%)
    pallas_call x1, Pallas kernels, body(): pl.pallas_call(functools.partial(kernel, size), out_shape=(jax.ShapeDtype...  87.1 us
    unnamed x2, local copies, waits for them, and re-layouts  3.5 us

commit v1 on v0

v1 whole, which is shorter than its diff:
```python
import functools

import jax
import jax.numpy as jnp
import numpy as np
from jax import lax
from jax.experimental import pallas as pl
from jax.experimental.pallas import tpu as pltpu
from jax.sharding import PartitionSpec as P

epsilon = 1e-06
rope_base = 10000.0
UNITS = 8
SPLIT = (4, 5, 6)
GROUPS = ((0,), (1,), (2,), (3,), (4, 5), (6,), (7,))
F32 = jnp.float32
BF16 = jnp.bfloat16
MESH = pl.DeviceIdType.MESH


def dot(a, b):
    return jnp.dot(a, b, preferred_element_type=F32)


def iota(shape, dim):
    return lax.broadcasted_iota(jnp.int32, shape, dim)


def silu(v):
    return v / (1.0 + jnp.exp(-v))


def kernel(
    size,
    tgain, ids_t, rweights_t, decay, hgain, freq, turn_sign,
    tok_h, wg_h, wu_h, query_h, key_h, value_h, gate_h, ow_h, wd_h,
    ret_out, exp_out,
    tok, wg, wu, query, key, value, gate, ow, wd,
    normed, obuf, xbuf, hbuf, sbuf, rbuf, w_hi, w_lo, cos_t, sin_t,
    rq, rk, local, state, total_state, st_send, st_recv, mixed, part, rs1, rs2_send, rs2_recv,
    load_sem, d_send, d_recv, xy_send, xy_recv, xc_send, xc_recv,
    hy_send, hy_recv, hc_send, hc_recv, b_send, b_recv, st_ssem, st_rsem,
    r1_send, r1_recv, r2_send, r2_recv,
):
    ep, tp, cap, rounds, per, groups = (
        size["ep"], size["tp"], size["cap"], size["rounds"], size["per"], size["groups"]
    )
    ys = tp // 2
    e, t = lax.axis_index("ep"), lax.axis_index("tp")
    y, c = t // 2, lax.rem(t, 2)
    mate = (e, y * 2 + 1 - c)
    heads = decay.shape[0]
    tokens, model = tok.shape
    half = model // 2
    block_len = query.shape[0]
    dk = query.shape[1] // heads

    def bit(b):
        return lax.rem(e // 2**b, 2)

    def flipped(k):
        out = e
        for b in range(rounds):
            if k >> b & 1:
                out = out + (1 - 2 * bit(b)) * 2**b
        return out

    def pair(k):
        return (flipped(k), t)

    def y_at(offset):
        return lax.rem(y + offset, ys)

    def over_y(offset):
        return (e, y_at(offset) * 2 + c)

    def remote(src, dst, ssem, rsem, device):
        return pltpu.make_async_remote_copy(
            src_ref=src, dst_ref=dst, send_sem=ssem, recv_sem=rsem,
            device_id=device, device_id_type=MESH,
        )

    sent = []

    def send(src, dst, ssem, rsem, device):
        copy = remote(src, dst, ssem, rsem, device)
        copy.start()
        sent.append(copy)

    def arrived(dst, ssem, rsem, device):
        remote(dst, dst, ssem, rsem, device).wait_recv()

    loads = {
        name: pltpu.make_async_copy(a, b, load_sem.at[i])
        for i, (name, a, b) in enumerate((
            ("tok", tok_h, tok), ("wg", wg_h, wg), ("wu", wu_h, wu), ("query", query_h, query),
            ("key", key_h, key), ("value", value_h, value), ("gate", gate_h, gate),
            ("ow", ow_h, ow), ("wd", wd_h, wd)))
    }
    for copy in loads.values():
        copy.start()

    barrier = pltpu.get_barrier_semaphore()
    friends = [pair(k) for k in range(1, ep)] + [over_y(i) for i in range(1, ys)] + [mate]
    for friend in friends:
        pl.semaphore_signal(barrier, inc=1, device_id=friend, device_id_type=MESH)

    rows = max(ep, 16)
    after = jnp.where(
        iota((tokens, tokens), 0) < iota((tokens, tokens), 1), 1.0, 0.0).astype(BF16)

    def positions(ids):
        rel = jnp.bitwise_xor(ids, e)
        named = [iota((rows, tokens), 0) == rel[i:i + 1, :] for i in range(2)]
        rank = dot(jnp.where(named[0] | named[1], 1.0, 0.0).astype(BF16), after)
        return [
            rel[i:i + 1, :] * cap + jnp.sum(
                jnp.where(named[i], rank, 0.0), 0, keepdims=True).astype(jnp.int32)
            for i in range(2)
        ]

    def picks(pos, k, n):
        row_id = k * cap + iota((n * cap, tokens), 0)
        return jnp.where((row_id == pos[0]) | (row_id == pos[1]), 1.0, 0.0).astype(BF16)

    pos_t = positions(ids_t[...])
    loads["tok"].wait()
    rows_float = tok[...].astype(F32)
    scale = lax.rsqrt(jnp.mean(rows_float * rows_float, -1, keepdims=True) + epsilon)
    normed[...] = (rows_float * scale * tgain[...]).astype(BF16)

    def block(j, n=1):
        return pl.ds(j * cap, n * cap)

    def unit(u, n=1):
        return block(u * per, n * per)

    mine = pl.ds(pl.multiple_of(c * half, half), half)
    def blocks(u):
        return [k for k in range(u * per, (u + 1) * per) if k > 0]

    quarter = half // ys

    def part_cols(i):
        return pl.ds(pl.multiple_of(i * quarter, quarter), quarter)

    def push(u):
        if u in SPLIT:
            cols, source = part_cols(y), pl.ds(
                pl.multiple_of(c * half + y * quarter, quarter), quarter)
        else:
            cols, source = pl.ds(0, half), mine
        obuf[unit(u), cols] = dot(picks(pos_t, u * per, per), normed[:, source]).astype(BF16)
        for k in blocks(u):
            send(obuf.at[block(k), cols], xbuf.at[c, block(k), cols], d_send.at[k], d_recv.at[k],
                 pair(k))

    def landed(u, cols):
        for k in blocks(u):
            arrived(xbuf.at[c, block(k), cols], d_send.at[k], d_recv.at[k], pair(k))

    def y_relay(u):
        landed(u, part_cols(y))
        for a in range(1, ys):
            ref = xbuf.at[c, unit(u), part_cols(y)]
            send(ref, ref, xy_send.at[a, u], xy_recv.at[a, u], over_y(a))

    def x_relay(u):
        if not blocks(u):
            return
        if u in SPLIT:
            for a in range(1, ys):
                arrived(xbuf.at[c, unit(u), part_cols(y_at(ys - a))], xy_send.at[a, u],
                        xy_recv.at[a, u], over_y(a))
        else:
            landed(u, pl.ds(0, half))
        send(xbuf.at[c, unit(u)], xbuf.at[c, unit(u)], xc_send.at[u], xc_recv.at[u], mate)

    def own_block():
        if per == 1:
            own = picks(pos_t, 0, 1)
            for i in range(2):
                xbuf[i, block(0), :] = dot(own, normed[:, pl.ds(i * half, half)]).astype(BF16)
        else:
            xbuf[c, block(0), :] = obuf[block(0), :]

    pl.semaphore_wait(barrier, len(friends))
    def x_collect(u):
        if not blocks(u):
            return
        arrived(xbuf.at[1 - c, unit(u)], xc_send.at[u], xc_recv.at[u], mate)

    ff = wg.shape[1]
    n_tile = min(256, ff)

    def group_rows(g):
        return unit(groups[g][0], len(groups[g]))

    def up(g):
        for u in groups[g]:
            x_collect(u)
        rws = group_rows(g)

        def tile(n, carry):
            cols = pl.ds(pl.multiple_of(n * n_tile, n_tile), n_tile)
            a = v = None
            for p in range(2):
                x = xbuf[p, rws, :]
                ins = pl.ds(p * half, half)
                gp, vp = dot(x, wg[ins, cols]), dot(x, wu[ins, cols])
                a, v = (gp, vp) if a is None else (a + gp, v + vp)
            hbuf[t, rws, cols] = (silu(a) * v).astype(BF16)
            return carry

        lax.fori_loop(0, ff // n_tile, tile, 0)
        for a in range(1, ys):
            send(hbuf.at[t, rws], hbuf.at[t, rws], hy_send.at[a, g], hy_recv.at[a, g], over_y(a))
        send(hbuf.at[t, rws], hbuf.at[t, rws], hc_send.at[0, g], hc_recv.at[0, g], mate)

    def h_pass(g):
        rws = group_rows(g)
        for a in range(1, ys):
            piece = y_at(ys - a) * 2 + c
            arrived(hbuf.at[piece, rws], hy_send.at[a, g], hy_recv.at[a, g], over_y(a))
            send(hbuf.at[piece, rws], hbuf.at[piece, rws], hc_send.at[a, g], hc_recv.at[a, g],
                 mate)

    cw = wd.shape[1]
    d_tile = min(256, cw)

    def down(g):
        rws = group_rows(g)
        for a in range(ys):
            piece = y_at(ys - a) * 2 + 1 - c
            arrived(hbuf.at[piece, rws], hc_send.at[a, g], hc_recv.at[a, g], mate)

        def tile(n, carry):
            cols = pl.ds(pl.multiple_of(n * d_tile, d_tile), d_tile)
            total = None
            for p in range(tp):
                now = dot(hbuf[p, rws, :], wd[pl.ds(p * ff, ff), cols])
                total = now if total is None else total + now
            sbuf[rws, cols] = total.astype(BF16)
            return carry

        lax.fori_loop(0, cw // d_tile, tile, 0)
        for u in groups[g]:
            for k in range(u * per, (u + 1) * per):
                if k > 0:
                    send(sbuf.at[block(k)], rbuf.at[block(k)], b_send.at[k], b_recv.at[k], pair(k))
                else:
                    rbuf[block(0), :] = sbuf[block(0), :]

    within = iota((block_len, 1), 0).astype(F32)

    def head_cols(h):
        return pl.ds(pl.multiple_of(h * dk, dk), dk)

    def turn(x):
        return x * cos_t[...] + pltpu.roll(x, dk // 2, 1) * sin_t[...]

    def states():
        for name in ("query", "key", "value"):
            loads[name].wait()
        angles = (e * block_len + iota((block_len, dk), 0)).astype(F32) * freq[...]
        cos_t[...] = jnp.cos(angles)
        sin_t[...] = jnp.sin(angles) * turn_sign[...]

        def one(h, carry):
            cols = head_cols(h)
            rate = decay[h]
            rq[:, cols] = turn(query[:, cols].astype(F32)).astype(BF16)
            rot_key = (turn(key[:, cols].astype(F32)) * dk ** (-0.5)).astype(BF16)
            rk[:, cols] = rot_key
            decayed = (rot_key.astype(F32) * jnp.exp(-rate * (block_len - 1.0 - within))).astype(BF16)
            now = lax.dot_general(
                decayed, value[:, cols], (((0,), (0,)), ((), ())), preferred_element_type=F32)
            total_state[h] = now
            state[h] = jnp.zeros((dk, dk), F32)
            return carry

        lax.fori_loop(0, heads, one, 0)

    def lane(h, times):
        return jnp.exp(jnp.full((1, dk), -decay[h] * (block_len * times), F32))

    last = rounds - 1

    def state_copy(r):
        return remote(st_send.at[r], st_recv.at[r], st_ssem.at[r], st_rsem.at[r], pair(2**r))

    def state_send(r):
        def one(h, carry):
            st_send[r, h] = total_state[h].astype(BF16)
            return carry

        lax.fori_loop(0, heads, one, 0)
        if r < last:
            copy = state_copy(r)
            copy.start()
            sent.append(copy)
        else:
            @pl.when(bit(r) == 0)
            def _():
                state_copy(r).start()

    def state_take(r):
        later = bit(r) == 1
        before = lax.rem(e, 2**r).astype(F32)

        def one(h, carry):
            got = st_recv[r, h].astype(F32)
            state[h] = state[h] + jnp.where(later, got * lane(h, before), 0.0)
            if r < last:
                far = lane(h, float(2**r))
                total_state[h] = jnp.where(
                    later, got * far + total_state[h], total_state[h] * far + got)
            return carry

        def take():
            state_copy(r).wait_recv()
            lax.fori_loop(0, heads, one, 0)

        if r < last:
            take()
        else:
            pl.when(later)(take)

    def combine_weights():
        diagonal = iota((tokens, tokens), 0) == iota((tokens, tokens), 1)

        def upright(row):
            return jnp.sum(jnp.where(diagonal, row, 0.0), 1, keepdims=True)

        col = iota((tokens, ep * cap), 1)
        pos0 = upright(pos_t[0].astype(F32)).astype(jnp.int32)
        pos1 = upright(pos_t[1].astype(F32)).astype(jnp.int32)
        weight = jnp.where(col == pos0, upright(rweights_t[0:1, :]), 0.0) + jnp.where(
            col == pos1, upright(rweights_t[1:2, :]), 0.0)
        high = weight.astype(BF16)
        w_hi[...] = high
        w_lo[...] = (weight - high.astype(F32)).astype(BF16)

    chunk = min(128, block_len)

    def head_local(first, last):
        def step(n, carry):
            h, i = n // (block_len // chunk), lax.rem(n, block_len // chunk)
            cols = head_cols(h)
            rate = decay[h]
            key_grow = jnp.exp(rate * iota((1, block_len), 1).astype(F32))
            rws = pl.ds(pl.multiple_of(i * chunk, chunk), chunk)
            place = i * chunk + iota((chunk, 1), 0)
            scores = lax.dot_general(
                rq[rws, cols], rk[:, cols], (((1,), (1,)), ((), ())), preferred_element_type=F32)
            fade = jnp.exp(-rate * place.astype(F32)) * key_grow
            seen = iota((chunk, block_len), 1) <= place
            weights = jnp.where(seen, scores * fade, 0.0).astype(BF16)
            local[rws, cols] = dot(weights, value[:, cols])
            return carry

        n = block_len // chunk
        lax.fori_loop(first * n, last * n, step, 0)

    def finish():
        def step(n, carry):
            h, i = n // (block_len // chunk), lax.rem(n, block_len // chunk)
            cols = head_cols(h)
            rws = pl.ds(pl.multiple_of(i * chunk, chunk), chunk)
            place = (i * chunk + iota((chunk, 1), 0)).astype(F32)
            held = state[h]
            high = held.astype(BF16)
            low = (held - high.astype(F32)).astype(BF16)
            q = rq[rws, cols]
            retained = local[rws, cols] + (dot(q, high) + dot(q, low)) * jnp.exp(
                -decay[h] * (place + 1.0))
            centered = retained - jnp.mean(retained, -1, keepdims=True)
            out = centered * lax.rsqrt(jnp.mean(centered * centered, -1, keepdims=True) + epsilon)
            mixed[rws, cols] = (
                out * hgain[:, cols] * silu(gate[rws, cols].astype(F32))).astype(BF16)
            return carry

        lax.fori_loop(0, heads * (block_len // chunk), step, 0)

    rb = block_len // tp
    o_tile = min(512, model)

    def project():
        def step(n, carry):
            cols = pl.ds(pl.multiple_of(n * o_tile, o_tile), o_tile)
            for d in range(tp):
                part[d, :, cols] = dot(mixed[pl.ds(d * rb, rb), :], ow[:, cols]).astype(BF16)
            return carry

        lax.fori_loop(0, model // o_tile, step, 0)
        for b in range(ys):
            send(part.at[b * 2 + 1 - c], rs1.at[b], r1_send.at[b], r1_recv.at[b], mate)

    def sum_over_cores():
        for b in range(ys):
            arrived(rs1.at[b], r1_send.at[b], r1_recv.at[b], mate)
        for a in range(1, ys):
            b = y_at(a)
            rs2_send[a - 1] = (part[b * 2 + c].astype(F32) + rs1[b].astype(F32)).astype(BF16)
            send(rs2_send.at[a - 1], rs2_recv.at[a - 1], r2_send.at[a - 1], r2_recv.at[a - 1],
                 over_y(a))

    if blocks(0):
        push(0)
    push(1)
    push(2)
    push(3)
    own_block()
    loads["wg"].wait()
    loads["wu"].wait()
    x_relay(0)
    up(0)
    states()
    state_send(0)
    push(4)
    push(5)
    x_relay(1)
    up(1)
    x_relay(2)
    h_pass(0)
    up(2)
    y_relay(4)
    x_relay(3)
    state_take(0)
    state_send(1)
    push(6)
    y_relay(5)
    up(3)
    h_pass(1)
    state_take(1)
    state_send(2)
    push(7)
    head_local(0, heads)
    h_pass(2)
    x_relay(4)
    x_relay(5)
    combine_weights()
    for r in range(3, rounds):
        state_take(r - 1)
        state_send(r)
    y_relay(6)
    up(4)
    h_pass(3)
    state_take(last)
    loads["gate"].wait()
    loads["ow"].wait()
    finish()
    x_relay(6)
    project()
    up(5)
    loads["wd"].wait()
    x_relay(7)
    h_pass(4)
    up(6)
    down(4)
    sum_over_cores()
    down(0)
    down(1)
    h_pass(5)
    down(2)
    down(3)
    down(5)
    h_pass(6)
    down(6)

    total = part[t].astype(F32) + rs1[y].astype(F32)
    for a in range(1, ys):
        arrived(rs2_recv.at[a - 1], r2_send.at[a - 1], r2_recv.at[a - 1], over_y(a))
        total += rs2_recv[a - 1].astype(F32)
    ret_out[...] = total.astype(BF16)
    for k in range(1, ep):
        arrived(rbuf.at[block(k)], b_send.at[k], b_recv.at[k], pair(k))
    exp_out[...] = (dot(w_hi[...], rbuf[...]) + dot(w_lo[...], rbuf[...])).astype(BF16)
    for copy in sent:
        copy.wait_send()

    @pl.when(bit(last) == 0)
    def _():
        state_copy(last).wait_send()


def body(
    query_in, key_in, value_in, gate_in, decay_rate, head_gain, output_weight,
    token_rows, token_gain, route_ids, route_weights, expert_gate, expert_up, expert_down,
):
    ep, tp = lax.axis_size("ep"), lax.axis_size("tp")
    tokens, model = token_rows.shape
    top = route_ids.shape[1]
    cap = -(-(2 * tokens * top // ep) // 32) * 32
    block_len, width = query_in.shape
    heads = decay_rate.shape[0]
    dk = width // heads
    ff = expert_gate.shape[2]
    cw = expert_down.shape[2]
    ys = tp // 2
    rounds = ep.bit_length() - 1
    assert ep == 2**rounds and rounds >= 3
    per = ep // UNITS
    turns = dk // 2
    freq = np.tile(
        np.float32(rope_base) ** (-np.arange(turns, dtype=np.float32) * np.float32(2.0 / dk)), 2)
    turn_sign = np.where(np.arange(dk) < turns, -1.0, 1.0)
    size = dict(ep=ep, tp=tp, cap=cap, rounds=rounds, per=per, groups=GROUPS)
    slots = ep * cap
    rb = block_len // tp
    vmem = pl.BlockSpec(memory_space=pltpu.VMEM)
    smem = pl.BlockSpec(memory_space=pltpu.SMEM)
    hbm = pl.BlockSpec(memory_space=pl.ANY)
    dma = pltpu.SemaphoreType.DMA
    big = [token_rows, expert_gate[0], expert_up[0], query_in, key_in, value_in, gate_in,
           output_weight, expert_down[0]]
    nm = len(GROUPS)
    return pl.pallas_call(
        functools.partial(kernel, size),
        out_shape=(
            jax.ShapeDtypeStruct((rb, model), BF16),
            jax.ShapeDtypeStruct((tokens, cw), BF16),
        ),
        in_specs=[vmem] * 3 + [smem] + [vmem] * 3 + [hbm] * 9,
        out_specs=(vmem, vmem),
        scratch_shapes=[pltpu.VMEM(a.shape, BF16) for a in big]
        + [
            pltpu.VMEM((tokens, model), BF16),
            pltpu.VMEM((slots, model // 2), BF16),
            pltpu.VMEM((2, slots, model // 2), BF16),
            pltpu.VMEM((tp, slots, ff), BF16),
            pltpu.VMEM((slots, cw), BF16),
            pltpu.VMEM((slots, cw), BF16),
            pltpu.VMEM((tokens, slots), BF16),
            pltpu.VMEM((tokens, slots), BF16),
            pltpu.VMEM((block_len, dk), F32),
            pltpu.VMEM((block_len, dk), F32),
            pltpu.VMEM((block_len, width), BF16),
            pltpu.VMEM((block_len, width), BF16),
            pltpu.VMEM((block_len, width), F32),
            pltpu.VMEM((heads, dk, dk), F32),
            pltpu.VMEM((heads, dk, dk), F32),
            pltpu.VMEM((rounds, heads, dk, dk), BF16),
            pltpu.VMEM((rounds, heads, dk, dk), BF16),
            pltpu.VMEM((block_len, width), BF16),
            pltpu.VMEM((tp, rb, model), BF16),
            pltpu.VMEM((ys, rb, model), BF16),
            pltpu.VMEM((max(ys - 1, 1), rb, model), BF16),
            pltpu.VMEM((max(ys - 1, 1), rb, model), BF16),
            dma((9,)),
            dma((ep,)), dma((ep,)),
            dma((ys, UNITS)), dma((ys, UNITS)), dma((UNITS,)), dma((UNITS,)),
            dma((ys, nm)), dma((ys, nm)), dma((ys, nm)), dma((ys, nm)),
            dma((ep,)), dma((ep,)),
            dma((rounds,)), dma((rounds,)),
            dma((ys,)), dma((ys,)), dma((ys,)), dma((ys,)),
        ],
        compiler_params=pltpu.CompilerParams(
            collective_id=0, has_side_effects=True, vmem_limit_bytes=60 * 2**20
        ),
    )(
        token_gain[None, :], route_ids.T, route_weights.T,
        decay_rate, head_gain[None, :],
        jnp.asarray(freq[None, :], F32), jnp.asarray(turn_sign[None, :], F32),
        *big,
    )


def solution(mesh):
    placed = (
        P("ep", "tp"), P("ep", "tp"), P("ep", "tp"), P("ep", "tp"),
        P("tp"), P("tp"), P("tp", None), P("ep", None), P(),
        P("ep", None), P("ep", None),
        P("ep", None, "tp"), P("ep", None, "tp"), P("ep", None, "tp"),
    )
    return jax.shard_map(
        body,
        mesh=mesh,
        in_specs=placed,
        out_specs=(P(("ep", "tp"), None), P("ep", "tp")),
        check_vma=False,
    )
```

time: 92.3 us -> 76.5 us (0.83)
  Pallas kernels: 87.1 us -> 71.6 us
    pallas_call x1, Pallas kernels: 87.1 us -> 71.6 us  [body(): pl.pallas_call(functools.partial(kernel, size), out_shape=(jax.ShapeDtype...]
where the time goes in v1:
time: 76.5 us; the launch traced here: 75.7 us
  Pallas kernels  71.6 us (94%)
  local copies, waits for them, and re-layouts  3.5 us (5%)
    pallas_call x1, Pallas kernels, body(): pl.pallas_call(functools.partial(kernel, size), out_shape=(jax.ShapeDtype...  71.6 us
    unnamed x2, local copies, waits for them, and re-layouts  3.5 us

profile of v1, /device:TPU:0, one launch (start us, length us, event | category | flops | bytes accessed | tf_op | source)
XLA Modules:
  0.0 75.7 jit_solution(15892522464739894920)
XLA Ops:
  0.6 71.6 %shard_map.167 = (bf16[128,2048]{1,0:T(8,128)(2,1)}, bf16[192,512]{1,0:T(8,128)(2,1)}) custom-call(f32[1,2048]{1,0:T(1,128)} %bitcast.10, s32[2,192]{1,0:T(2,128)} %bitcast.11, f32[2,192]{1,0:T(2,128)} %bitcast.12, f32[4]{0:T(128)} %decay.1, f32[1,512]{1,0:T(1,128)} %bitcast.13, f32[1,128]{1,0:T(1,128)} %constant.4.clone.freq, ...), custom_call_target="tpu_custom_call" | custom-call | tf_op jit(solution)/shard_map/pallas_call | solution.py:518
  72.2 1.9 %copy.20 = bf16[128,2048]{1,0:T(8,128)(2,1)} copy(bf16[128,2048]{1,0:T(8,128)(2,1)} %get-tuple-element.4) | data formatting | bytes 1048576
  74.1 1.6 %copy.21 = bf16[192,512]{1,0:T(8,128)(2,1)} copy(bf16[192,512]{1,0:T(8,128)(2,1)} %get-tuple-element.5) | data formatting | bytes 393216

commit v2 on v1

--- a/solution.py
+++ b/solution.py
@@ -10,9 +10,8 @@
 
 epsilon = 1e-06
 rope_base = 10000.0
-UNITS = 8
-SPLIT = (4, 5, 6)
-GROUPS = ((0,), (1,), (2,), (3,), (4, 5), (6,), (7,))
+UNITS, PIECES = 8, 2
+GROUPS = tuple((u,) for u in range(UNITS))
 F32 = jnp.float32
 BF16 = jnp.bfloat16
 MESH = pl.DeviceIdType.MESH
@@ -32,15 +31,16 @@
 
 def kernel(
     size,
-    tgain, ids_t, rweights_t, decay, hgain, freq, turn_sign,
-    tok_h, wg_h, wu_h, query_h, key_h, value_h, gate_h, ow_h, wd_h,
+    ids_h, tok_h, tgain_h, wg_h, wu_h, query_h, key_h, value_h, decay_h, freq_h, sign_h,
+    rweights_h, gate_h, hgain_h, ow_h, wd_h,
     ret_out, exp_out,
-    tok, wg, wu, query, key, value, gate, ow, wd,
-    normed, obuf, xbuf, hbuf, sbuf, rbuf, w_hi, w_lo, cos_t, sin_t,
+    ids_t, tok, tgain, wg, wu, query, key, value, decay, freq, turn_sign,
+    rweights_t, gate, hgain, ow, wd,
+    normed, raw, ids_in, far_picks, obuf, xbuf, hbuf, gate_acc, up_acc, sbuf, rbuf, w_hi, w_lo, cos_t, sin_t,
     rq, rk, local, state, total_state, st_send, st_recv, mixed, part, rs1, rs2_send, rs2_recv,
-    load_sem, d_send, d_recv, xy_send, xy_recv, xc_send, xc_recv,
+    load_sem, id_send, id_recv, raw_send, raw_recv, ry_send, ry_recv, d_send, d_recv, xc_send, xc_recv,
     hy_send, hy_recv, hc_send, hc_recv, b_send, b_recv, st_ssem, st_rsem,
-    r1_send, r1_recv, r2_send, r2_recv,
+    r1_send, r1_recv, r2_send, r2_recv, ret, exp, out_sem,
 ):
     ep, tp, cap, rounds, per, groups = (
         size["ep"], size["tp"], size["cap"], size["rounds"], size["per"], size["groups"]
@@ -93,9 +93,11 @@
     loads = {
         name: pltpu.make_async_copy(a, b, load_sem.at[i])
         for i, (name, a, b) in enumerate((
-            ("tok", tok_h, tok), ("wg", wg_h, wg), ("wu", wu_h, wu), ("query", query_h, query),
-            ("key", key_h, key), ("value", value_h, value), ("gate", gate_h, gate),
-            ("ow", ow_h, ow), ("wd", wd_h, wd)))
+            ("ids", ids_h, ids_t), ("tok", tok_h, tok), ("tgain", tgain_h, tgain),
+            ("wg", wg_h, wg), ("wu", wu_h, wu), ("query", query_h, query), ("key", key_h, key),
+            ("value", value_h, value), ("decay", decay_h, decay), ("freq", freq_h, freq),
+            ("sign", sign_h, turn_sign), ("rweights", rweights_h, rweights_t),
+            ("gate", gate_h, gate), ("hgain", hgain_h, hgain), ("ow", ow_h, ow), ("wd", wd_h, wd)))
     }
     for copy in loads.values():
         copy.start()
@@ -123,8 +125,10 @@
         row_id = k * cap + iota((n * cap, tokens), 0)
         return jnp.where((row_id == pos[0]) | (row_id == pos[1]), 1.0, 0.0).astype(BF16)
 
+    loads["ids"].wait()
     pos_t = positions(ids_t[...])
     loads["tok"].wait()
+    loads["tgain"].wait()
     rows_float = tok[...].astype(F32)
     scale = lax.rsqrt(jnp.mean(rows_float * rows_float, -1, keepdims=True) + epsilon)
     normed[...] = (rows_float * scale * tgain[...]).astype(BF16)
@@ -139,41 +143,67 @@
     def blocks(u):
         return [k for k in range(u * per, (u + 1) * per) if k > 0]
 
-    quarter = half // ys
-
-    def part_cols(i):
-        return pl.ds(pl.multiple_of(i * quarter, quarter), quarter)
+    units = ep // per
+    far, near = ep // 2, units // 2
+    pieces = size["pieces"]
+    width = half // pieces
+    strip = width // ys
+
+    def piece(i):
+        return pl.ds(i * width, width)
+
+    def strip_cols(i, at):
+        return pl.ds(pl.multiple_of(i * width + at * strip, strip), strip)
 
     def push(u):
-        if u in SPLIT:
-            cols, source = part_cols(y), pl.ds(
-                pl.multiple_of(c * half + y * quarter, quarter), quarter)
-        else:
-            cols, source = pl.ds(0, half), mine
-        obuf[unit(u), cols] = dot(picks(pos_t, u * per, per), normed[:, source]).astype(BF16)
+        obuf[unit(u), :] = dot(picks(pos_t, u * per, per), normed[:, mine]).astype(BF16)
         for k in blocks(u):
-            send(obuf.at[block(k), cols], xbuf.at[c, block(k), cols], d_send.at[k], d_recv.at[k],
+            send(obuf.at[block(k)], xbuf.at[c, block(k)], d_send.at[k, 0], d_recv.at[k, 0],
                  pair(k))
 
-    def landed(u, cols):
+    def raw_push(i):
+        if i == 0:
+            send(ids_t, ids_in, id_send.at[0], id_recv.at[0], pair(far))
+        cols = pl.ds(pl.multiple_of(c * half + i * width + y * strip, strip), strip)
+        send(normed.at[:, cols], raw.at[:, strip_cols(i, y)], raw_send.at[i], raw_recv.at[i],
+             pair(far))
+
+    def raw_relay(i):
+        ref = raw.at[:, strip_cols(i, y)]
+        arrived(ref, raw_send.at[i], raw_recv.at[i], pair(far))
+        for a in range(1, ys):
+            send(ref, ref, ry_send.at[a, i], ry_recv.at[a, i], over_y(a))
+
+    def far_select(i):
+        if i == 0:
+            arrived(ids_in, id_send.at[0], id_recv.at[0], pair(far))
+            far_picks[...] = picks(positions(ids_in[...]), 0, far)
+        for a in range(1, ys):
+            arrived(raw.at[:, strip_cols(i, y_at(ys - a))], ry_send.at[a, i], ry_recv.at[a, i],
+                    over_y(a))
+        for u in range(near):
+            chosen = dot(far_picks[unit(u), :], raw[:, piece(i)]).astype(BF16)
+            obuf[unit(near + u), piece(i)] = chosen
+            if u == 0:
+                xbuf[c, block(far), piece(i)] = chosen[:cap]
+            for k in blocks(u):
+                j = far + k
+                send(obuf.at[block(j), piece(i)], xbuf.at[c, block(j), piece(i)],
+                     d_send.at[j, i], d_recv.at[j, i], pair(k))
+
+    def landed(u):
         for k in blocks(u):
-            arrived(xbuf.at[c, block(k), cols], d_send.at[k], d_recv.at[k], pair(k))
-
-    def y_relay(u):
-        landed(u, part_cols(y))
-        for a in range(1, ys):
-            ref = xbuf.at[c, unit(u), part_cols(y)]
-            send(ref, ref, xy_send.at[a, u], xy_recv.at[a, u], over_y(a))
+            if k < far:
+                arrived(xbuf.at[c, block(k)], d_send.at[k, 0], d_recv.at[k, 0], pair(k))
+            elif k > far:
+                for i in range(pieces):
+                    arrived(xbuf.at[c, block(k), piece(i)], d_send.at[k, i], d_recv.at[k, i],
+                            pair(k - far))
 
     def x_relay(u):
         if not blocks(u):
             return
-        if u in SPLIT:
-            for a in range(1, ys):
-                arrived(xbuf.at[c, unit(u), part_cols(y_at(ys - a))], xy_send.at[a, u],
-                        xy_recv.at[a, u], over_y(a))
-        else:
-            landed(u, pl.ds(0, half))
+        landed(u)
         send(xbuf.at[c, unit(u)], xbuf.at[c, unit(u)], xc_send.at[u], xc_recv.at[u], mate)
 
     def own_block():
@@ -213,6 +243,43 @@
             return carry
 
         lax.fori_loop(0, ff // n_tile, tile, 0)
+
+    def up_half(g, core):
+        ins = pl.ds(pl.multiple_of(core * half, half), half)
+        rws = group_rows(g)
+
+        def products(n):
+            cols = pl.ds(pl.multiple_of(n * n_tile, n_tile), n_tile)
+            x = xbuf[core, rws, :]
+            return cols, dot(x, wg[ins, cols]), dot(x, wu[ins, cols])
+
+        return rws, products
+
+    def up_mine(g):
+        rws, products = up_half(g, c)
+
+        def tile(n, carry):
+            cols, a, v = products(n)
+            gate_acc[:, cols] = a
+            up_acc[:, cols] = v
+            return carry
+
+        lax.fori_loop(0, ff // n_tile, tile, 0)
+
+    def up_rest(g):
+        for u in groups[g]:
+            x_collect(u)
+        rws, products = up_half(g, 1 - c)
+
+        def tile(n, carry):
+            cols, a, v = products(n)
+            hbuf[t, rws, cols] = (silu(gate_acc[:, cols] + a) * (up_acc[:, cols] + v)).astype(BF16)
+            return carry
+
+        lax.fori_loop(0, ff // n_tile, tile, 0)
+
+    def up_send(g):
+        rws = group_rows(g)
         for a in range(1, ys):
             send(hbuf.at[t, rws], hbuf.at[t, rws], hy_send.at[a, g], hy_recv.at[a, g], over_y(a))
         send(hbuf.at[t, rws], hbuf.at[t, rws], hc_send.at[0, g], hc_recv.at[0, g], mate)
@@ -260,7 +327,7 @@
         return x * cos_t[...] + pltpu.roll(x, dk // 2, 1) * sin_t[...]
 
     def states():
-        for name in ("query", "key", "value"):
+        for name in ("query", "key", "value", "decay", "freq", "sign"):
             loads[name].wait()
         angles = (e * block_len + iota((block_len, dk), 0)).astype(F32) * freq[...]
         cos_t[...] = jnp.cos(angles)
@@ -343,44 +410,48 @@
 
     chunk = min(128, block_len)
 
-    def head_local(first, last):
-        def step(n, carry):
-            h, i = n // (block_len // chunk), lax.rem(n, block_len // chunk)
+    chunks = block_len // chunk
+
+    def head_local(first, stop):
+        def one(h, carry):
             cols = head_cols(h)
             rate = decay[h]
             key_grow = jnp.exp(rate * iota((1, block_len), 1).astype(F32))
-            rws = pl.ds(pl.multiple_of(i * chunk, chunk), chunk)
-            place = i * chunk + iota((chunk, 1), 0)
-            scores = lax.dot_general(
-                rq[rws, cols], rk[:, cols], (((1,), (1,)), ((), ())), preferred_element_type=F32)
-            fade = jnp.exp(-rate * place.astype(F32)) * key_grow
-            seen = iota((chunk, block_len), 1) <= place
-            weights = jnp.where(seen, scores * fade, 0.0).astype(BF16)
-            local[rws, cols] = dot(weights, value[:, cols])
-            return carry
-
-        n = block_len // chunk
-        lax.fori_loop(first * n, last * n, step, 0)
-
-    def finish():
-        def step(n, carry):
-            h, i = n // (block_len // chunk), lax.rem(n, block_len // chunk)
+            for i in range(chunks):
+                seen_keys = (i + 1) * chunk
+                rws, keys = pl.ds(i * chunk, chunk), pl.ds(0, seen_keys)
+                place = i * chunk + iota((chunk, 1), 0)
+                scores = lax.dot_general(
+                    rq[rws, cols], rk[keys, cols], (((1,), (1,)), ((), ())),
+                    preferred_element_type=F32)
+                fade = jnp.exp(-rate * place.astype(F32)) * key_grow[:, :seen_keys]
+                seen = iota((chunk, seen_keys), 1) <= place
+                weights = jnp.where(seen, scores * fade, 0.0).astype(BF16)
+                local[rws, cols] = dot(weights, value[keys, cols])
+            return carry
+
+        lax.fori_loop(first, stop, one, 0)
+
+    def finish(first, stop):
+        def one(h, carry):
             cols = head_cols(h)
-            rws = pl.ds(pl.multiple_of(i * chunk, chunk), chunk)
-            place = (i * chunk + iota((chunk, 1), 0)).astype(F32)
             held = state[h]
             high = held.astype(BF16)
             low = (held - high.astype(F32)).astype(BF16)
-            q = rq[rws, cols]
-            retained = local[rws, cols] + (dot(q, high) + dot(q, low)) * jnp.exp(
-                -decay[h] * (place + 1.0))
-            centered = retained - jnp.mean(retained, -1, keepdims=True)
-            out = centered * lax.rsqrt(jnp.mean(centered * centered, -1, keepdims=True) + epsilon)
-            mixed[rws, cols] = (
-                out * hgain[:, cols] * silu(gate[rws, cols].astype(F32))).astype(BF16)
-            return carry
-
-        lax.fori_loop(0, heads * (block_len // chunk), step, 0)
+            for i in range(chunks):
+                rws = pl.ds(i * chunk, chunk)
+                place = (i * chunk + iota((chunk, 1), 0)).astype(F32)
+                q = rq[rws, cols]
+                retained = local[rws, cols] + (dot(q, high) + dot(q, low)) * jnp.exp(
+                    -decay[h] * (place + 1.0))
+                centered = retained - jnp.mean(retained, -1, keepdims=True)
+                out = centered * lax.rsqrt(
+                    jnp.mean(centered * centered, -1, keepdims=True) + epsilon)
+                mixed[rws, cols] = (
+                    out * hgain[:, cols] * silu(gate[rws, cols].astype(F32))).astype(BF16)
+            return carry
+
+        lax.fori_loop(first, stop, one, 0)
 
     rb = block_len // tp
     o_tile = min(512, model)
@@ -407,81 +478,127 @@
 
     if blocks(0):
         push(0)
-    push(1)
-    push(2)
-    push(3)
+    for u in range(1, near):
+        push(u)
     own_block()
     loads["wg"].wait()
     loads["wu"].wait()
     x_relay(0)
     up(0)
+    up_send(0)
     states()
+    for i in range(pieces):
+        raw_push(i)
     state_send(0)
-    push(4)
-    push(5)
     x_relay(1)
-    up(1)
+    up_mine(1)
     x_relay(2)
+    up_rest(1)
+    up_send(1)
     h_pass(0)
+    head_local(0, heads)
+    raw_relay(0)
     up(2)
-    y_relay(4)
-    x_relay(3)
+    for i in range(1, pieces):
+        raw_relay(i)
+    up_send(2)
     state_take(0)
     state_send(1)
-    push(6)
-    y_relay(5)
+    x_relay(3)
+    h_pass(1)
+    far_select(0)
     up(3)
-    h_pass(1)
+    up_send(3)
+    loads["wd"].wait()
+    down(0)
+    for i in range(1, pieces):
+        far_select(i)
+    x_relay(4)
+    up_mine(4)
     state_take(1)
     state_send(2)
-    push(7)
-    head_local(0, heads)
     h_pass(2)
-    x_relay(4)
+    up_rest(4)
+    up_send(4)
     x_relay(5)
-    combine_weights()
+    x_relay(6)
+    h_pass(3)
+    down(1)
+    up(5)
+    up_send(5)
     for r in range(3, rounds):
         state_take(r - 1)
         state_send(r)
-    y_relay(6)
-    up(4)
-    h_pass(3)
+    x_relay(7)
     state_take(last)
     loads["gate"].wait()
+    loads["hgain"].wait()
     loads["ow"].wait()
-    finish()
-    x_relay(6)
-    project()
-    up(5)
-    loads["wd"].wait()
-    x_relay(7)
+    finish(0, heads)
     h_pass(4)
     up(6)
+    up_send(6)
+    project()
+    up(7)
+    up_send(7)
+    early = len(sent)
+    h_pass(5)
+    sum_over_cores()
     down(4)
-    sum_over_cores()
-    down(0)
-    down(1)
-    h_pass(5)
-    down(2)
-    down(3)
     down(5)
     h_pass(6)
+    down(2)
     down(6)
-
+    down(3)
+    loads["rweights"].wait()
+    combine_weights()
+    h_pass(7)
+    down(7)
+
+    for copy in sent[:early]:
+        copy.wait_send()
+    split = ep // 2
+    for k in range(1, split):
+        arrived(rbuf.at[block(k)], b_send.at[k], b_recv.at[k], pair(k))
+
+    def weighed(cols):
+        rows_back = rbuf[cols, :]
+        return dot(w_hi[:, cols], rows_back) + dot(w_lo[:, cols], rows_back)
+
+    close = weighed(block(0, split))
     total = part[t].astype(F32) + rs1[y].astype(F32)
     for a in range(1, ys):
         arrived(rs2_recv.at[a - 1], r2_send.at[a - 1], r2_recv.at[a - 1], over_y(a))
         total += rs2_recv[a - 1].astype(F32)
-    ret_out[...] = total.astype(BF16)
-    for k in range(1, ep):
+    ret[...] = total.astype(BF16)
+    ret_store = pltpu.make_async_copy(ret, ret_out, out_sem.at[0])
+    ret_store.start()
+    for k in range(split, ep):
         arrived(rbuf.at[block(k)], b_send.at[k], b_recv.at[k], pair(k))
-    exp_out[...] = (dot(w_hi[...], rbuf[...]) + dot(w_lo[...], rbuf[...])).astype(BF16)
-    for copy in sent:
+    exp[...] = (close + weighed(block(split, ep - split))).astype(BF16)
+    exp_store = pltpu.make_async_copy(exp, exp_out, out_sem.at[1])
+    exp_store.start()
+    for copy in sent[early:]:
         copy.wait_send()
+    ret_store.wait()
+    exp_store.wait()
 
     @pl.when(bit(last) == 0)
     def _():
         state_copy(last).wait_send()
+
+
+def hand_on(ret_in, exp_in, ret_out, exp_out, ret, exp, in_sem, out_sem):
+    ways = ((ret_in, ret, ret_out), (exp_in, exp, exp_out))
+    taken = [pltpu.make_async_copy(a, b, in_sem.at[i]) for i, (a, b, _) in enumerate(ways)]
+    given = [pltpu.make_async_copy(b, d, out_sem.at[i]) for i, (_, b, d) in enumerate(ways)]
+    for copy in taken:
+        copy.start()
+    for i in range(2):
+        taken[i].wait()
+        given[i].start()
+    for copy in given:
+        copy.wait()
 
 
 def body(
@@ -501,34 +618,43 @@
     rounds = ep.bit_length() - 1
     assert ep == 2**rounds and rounds >= 3
     per = ep // UNITS
+    pieces = max(1, min(PIECES, model // (2 * 128 * ys)))
     turns = dk // 2
     freq = np.tile(
         np.float32(rope_base) ** (-np.arange(turns, dtype=np.float32) * np.float32(2.0 / dk)), 2)
     turn_sign = np.where(np.arange(dk) < turns, -1.0, 1.0)
-    size = dict(ep=ep, tp=tp, cap=cap, rounds=rounds, per=per, groups=GROUPS)
+    size = dict(ep=ep, tp=tp, cap=cap, rounds=rounds, per=per, groups=GROUPS, pieces=pieces)
     slots = ep * cap
     rb = block_len // tp
-    vmem = pl.BlockSpec(memory_space=pltpu.VMEM)
-    smem = pl.BlockSpec(memory_space=pltpu.SMEM)
     hbm = pl.BlockSpec(memory_space=pl.ANY)
     dma = pltpu.SemaphoreType.DMA
-    big = [token_rows, expert_gate[0], expert_up[0], query_in, key_in, value_in, gate_in,
-           output_weight, expert_down[0]]
+    given = [
+        route_ids.T, token_rows, token_gain[None, :], expert_gate[0], expert_up[0],
+        query_in, key_in, value_in, decay_rate,
+        jnp.asarray(freq[None, :], F32), jnp.asarray(turn_sign[None, :], F32),
+        route_weights.T, gate_in, head_gain[None, :], output_weight, expert_down[0],
+    ]
     nm = len(GROUPS)
-    return pl.pallas_call(
+    outs = pl.pallas_call(
         functools.partial(kernel, size),
         out_shape=(
             jax.ShapeDtypeStruct((rb, model), BF16),
             jax.ShapeDtypeStruct((tokens, cw), BF16),
         ),
-        in_specs=[vmem] * 3 + [smem] + [vmem] * 3 + [hbm] * 9,
-        out_specs=(vmem, vmem),
-        scratch_shapes=[pltpu.VMEM(a.shape, BF16) for a in big]
+        in_specs=[hbm] * len(given),
+        out_specs=(hbm, hbm),
+        scratch_shapes=[
+            (pltpu.SMEM if a is decay_rate else pltpu.VMEM)(a.shape, a.dtype) for a in given]
         + [
             pltpu.VMEM((tokens, model), BF16),
+            pltpu.VMEM((tokens, model // 2), BF16),
+            pltpu.VMEM((top, tokens), jnp.int32),
+            pltpu.VMEM((slots // 2, tokens), BF16),
             pltpu.VMEM((slots, model // 2), BF16),
             pltpu.VMEM((2, slots, model // 2), BF16),
             pltpu.VMEM((tp, slots, ff), BF16),
+            pltpu.VMEM((per * cap, ff), F32),
+            pltpu.VMEM((per * cap, ff), F32),
             pltpu.VMEM((slots, cw), BF16),
             pltpu.VMEM((slots, cw), BF16),
             pltpu.VMEM((tokens, slots), BF16),
@@ -547,23 +673,30 @@
             pltpu.VMEM((ys, rb, model), BF16),
             pltpu.VMEM((max(ys - 1, 1), rb, model), BF16),
             pltpu.VMEM((max(ys - 1, 1), rb, model), BF16),
-            dma((9,)),
-            dma((ep,)), dma((ep,)),
-            dma((ys, UNITS)), dma((ys, UNITS)), dma((UNITS,)), dma((UNITS,)),
+            dma((len(given),)),
+            dma((1,)), dma((1,)), dma((pieces,)), dma((pieces,)),
+            dma((ys, pieces)), dma((ys, pieces)),
+            dma((ep, pieces)), dma((ep, pieces)),
+            dma((UNITS,)), dma((UNITS,)),
             dma((ys, nm)), dma((ys, nm)), dma((ys, nm)), dma((ys, nm)),
             dma((ep,)), dma((ep,)),
             dma((rounds,)), dma((rounds,)),
             dma((ys,)), dma((ys,)), dma((ys,)), dma((ys,)),
+            pltpu.VMEM((rb, model), BF16),
+            pltpu.VMEM((tokens, cw), BF16),
+            dma((2,)),
         ],
         compiler_params=pltpu.CompilerParams(
             collective_id=0, has_side_effects=True, vmem_limit_bytes=60 * 2**20
         ),
-    )(
-        token_gain[None, :], route_ids.T, route_weights.T,
-        decay_rate, head_gain[None, :],
-        jnp.asarray(freq[None, :], F32), jnp.asarray(turn_sign[None, :], F32),
-        *big,
-    )
+    )(*given)
+    return pl.pallas_call(
+        hand_on,
+        out_shape=tuple(jax.ShapeDtypeStruct(a.shape, a.dtype) for a in outs),
+        in_specs=[hbm] * 2,
+        out_specs=(hbm, hbm),
+        scratch_shapes=[pltpu.VMEM(a.shape, a.dtype) for a in outs] + [dma((2,)), dma((2,))],
+    )(*outs)
 
 
 def solution(mesh):

time: 76.5 us -> 69.9 us (0.914)
  local copies, waits for them, and re-layouts: 3.5 us -> 0 us
  Pallas kernels: 71.6 us -> 68.9 us
    pallas_call x1, Pallas kernels: 71.6 us -> 67 us  [body(): pl.pallas_call(functools.partial(kernel, size), out_shape=(jax.ShapeDtype...]
    unnamed x2 -> x0, local copies, waits for them, and re-layouts: 3.5 us -> none
    pallas_call x0 -> x1, Pallas kernels: none -> 1.92 us  [body(): pl.pallas_call(hand_on, out_shape=tuple((jax.ShapeDtypeStruct(a.shape, a....]
where the time goes in v2:
time: 69.9 us; the launch traced here: 69.6 us
  Pallas kernels  68.9 us (99%)
    pallas_call x1, Pallas kernels, body(): pl.pallas_call(functools.partial(kernel, size), out_shape=(jax.ShapeDtype...  67 us
    pallas_call x1, Pallas kernels, body(): pl.pallas_call(hand_on, out_shape=tuple((jax.ShapeDtypeStruct(a.shape, a....  1.92 us

profile of v2, /device:TPU:0, one launch (start us, length us, event | category | flops | bytes accessed | tf_op | source)
XLA Modules:
  0.0 69.6 jit_solution(15557668556558719680)
XLA Ops:
  0.6 67.0 %shard_map.167 = (bf16[128,2048]{1,0:T(8,128)(2,1)}, bf16[192,512]{1,0:T(8,128)(2,1)}) custom-call(s32[2,192]{1,0:T(2,128)} %bitcast.11, bf16[192,2048]{1,0:T(8,128)(2,1)} %tok_h.1, f32[1,2048]{1,0:T(1,128)} %bitcast.10, bf16[2048,1024]{1,0:T(8,128)(2,1)} %bitcast.7, bf16[2048,1024]{1,0:T(8,128)(2,1)} %bitcast.8, bf16[512,512]{1,0:T(8,128)(2,1)} %query_h.1, ...), custom_call_target="tpu_custom_call" | custom-call | tf_op jit(solution)/shard_map/pallas_call | solution.py:638
  67.6 1.9 %shard_map.168 = (bf16[128,2048]{1,0:T(8,128)(2,1)}, bf16[192,512]{1,0:T(8,128)(2,1)}) custom-call(bf16[128,2048]{1,0:T(8,128)(2,1)} %get-tuple-element.4.ret_in, bf16[192,512]{1,0:T(8,128)(2,1)} %get-tuple-element.5.exp_in), custom_call_target="tpu_custom_call" | custom-call | tf_op jit(solution)/shard_map/pallas_call | solution.py:693

commit v3 on v2

--- a/solution.py
+++ b/solution.py
@@ -10,7 +10,8 @@
 
 epsilon = 1e-06
 rope_base = 10000.0
-UNITS, PIECES = 8, 2
+VMEM_LIMIT = 56 * 2**20
+UNITS, PIECES, SHARES = 8, 2, 2
 GROUPS = tuple((u,) for u in range(UNITS))
 F32 = jnp.float32
 BF16 = jnp.bfloat16
@@ -40,7 +41,7 @@
     rq, rk, local, state, total_state, st_send, st_recv, mixed, part, rs1, rs2_send, rs2_recv,
     load_sem, id_send, id_recv, raw_send, raw_recv, ry_send, ry_recv, d_send, d_recv, xc_send, xc_recv,
     hy_send, hy_recv, hc_send, hc_recv, b_send, b_recv, st_ssem, st_rsem,
-    r1_send, r1_recv, r2_send, r2_recv, ret, exp, out_sem,
+    r1_send, r1_recv, r2_send, r2_recv,
 ):
     ep, tp, cap, rounds, per, groups = (
         size["ep"], size["tp"], size["cap"], size["rounds"], size["per"], size["groups"]
@@ -90,11 +91,14 @@
     def arrived(dst, ssem, rsem, device):
         remote(dst, dst, ssem, rsem, device).wait_recv()
 
+    low, top = (pl.ds(i * (wg.shape[1] // 2), wg.shape[1] // 2) for i in range(2))
     loads = {
         name: pltpu.make_async_copy(a, b, load_sem.at[i])
         for i, (name, a, b) in enumerate((
             ("ids", ids_h, ids_t), ("tok", tok_h, tok), ("tgain", tgain_h, tgain),
-            ("wg", wg_h, wg), ("wu", wu_h, wu), ("query", query_h, query), ("key", key_h, key),
+            ("wg0", wg_h.at[:, low], wg.at[:, low]), ("wu0", wu_h.at[:, low], wu.at[:, low]),
+            ("wg1", wg_h.at[:, top], wg.at[:, top]), ("wu1", wu_h.at[:, top], wu.at[:, top]),
+            ("query", query_h, query), ("key", key_h, key),
             ("value", value_h, value), ("decay", decay_h, decay), ("freq", freq_h, freq),
             ("sign", sign_h, turn_sign), ("rweights", rweights_h, rweights_t),
             ("gate", gate_h, gate), ("hgain", hgain_h, hgain), ("ow", ow_h, ow), ("wd", wd_h, wd)))
@@ -146,6 +150,7 @@
     units = ep // per
     far, near = ep // 2, units // 2
     pieces = size["pieces"]
+    shares = min(SHARES, pieces)
     width = half // pieces
     strip = width // ys
 
@@ -164,11 +169,16 @@
     def raw_push(i):
         if i == 0:
             send(ids_t, ids_in, id_send.at[0], id_recv.at[0], pair(far))
-        cols = pl.ds(pl.multiple_of(c * half + i * width + y * strip, strip), strip)
-        send(normed.at[:, cols], raw.at[:, strip_cols(i, y)], raw_send.at[i], raw_recv.at[i],
-             pair(far))
+        shared = i < shares
+        begin = c * half + i * width + (y * strip if shared else 0)
+        size_of = strip if shared else width
+        cols = pl.ds(pl.multiple_of(begin, size_of), size_of)
+        there = strip_cols(i, y) if shared else piece(i)
+        send(normed.at[:, cols], raw.at[:, there], raw_send.at[i], raw_recv.at[i], pair(far))
 
     def raw_relay(i):
+        if i >= shares:
+            return
         ref = raw.at[:, strip_cols(i, y)]
         arrived(ref, raw_send.at[i], raw_recv.at[i], pair(far))
         for a in range(1, ys):
@@ -178,7 +188,9 @@
         if i == 0:
             arrived(ids_in, id_send.at[0], id_recv.at[0], pair(far))
             far_picks[...] = picks(positions(ids_in[...]), 0, far)
-        for a in range(1, ys):
+        if i >= shares:
+            arrived(raw.at[:, piece(i)], raw_send.at[i], raw_recv.at[i], pair(far))
+        for a in range(1, ys if i < shares else 1):
             arrived(raw.at[:, strip_cols(i, y_at(ys - a))], ry_send.at[a, i], ry_recv.at[a, i],
                     over_y(a))
         for u in range(near):
@@ -221,12 +233,12 @@
         arrived(xbuf.at[1 - c, unit(u)], xc_send.at[u], xc_recv.at[u], mate)
 
     ff = wg.shape[1]
-    n_tile = min(256, ff)
+    n_tile = min(256, ff // 2)
 
     def group_rows(g):
         return unit(groups[g][0], len(groups[g]))
 
-    def up(g):
+    def up(g, first=0, stop=None):
         for u in groups[g]:
             x_collect(u)
         rws = group_rows(g)
@@ -242,7 +254,7 @@
             hbuf[t, rws, cols] = (silu(a) * v).astype(BF16)
             return carry
 
-        lax.fori_loop(0, ff // n_tile, tile, 0)
+        lax.fori_loop(first, ff // n_tile if stop is None else stop, tile, 0)
 
     def up_half(g, core):
         ins = pl.ds(pl.multiple_of(core * half, half), half)
@@ -481,16 +493,25 @@
     for u in range(1, near):
         push(u)
     own_block()
-    loads["wg"].wait()
-    loads["wu"].wait()
+    loads["wg0"].wait()
+    loads["wu0"].wait()
     x_relay(0)
-    up(0)
+    parts = ff // n_tile
+    if blocks(0):
+        loads["wg1"].wait()
+        loads["wu1"].wait()
+        up(0)
+    else:
+        up(0, 0, parts // 2)
+        loads["wg1"].wait()
+        loads["wu1"].wait()
+        up(0, parts // 2, parts)
     up_send(0)
     states()
+    state_send(0)
+    x_relay(1)
     for i in range(pieces):
         raw_push(i)
-    state_send(0)
-    x_relay(1)
     up_mine(1)
     x_relay(2)
     up_rest(1)
@@ -522,10 +543,10 @@
     up_send(4)
     x_relay(5)
     x_relay(6)
-    h_pass(3)
     down(1)
     up(5)
     up_send(5)
+    h_pass(3)
     for r in range(3, rounds):
         state_take(r - 1)
         state_send(r)
@@ -535,16 +556,16 @@
     loads["hgain"].wait()
     loads["ow"].wait()
     finish(0, heads)
-    h_pass(4)
     up(6)
     up_send(6)
+    h_pass(4)
     project()
     up(7)
     up_send(7)
     early = len(sent)
+    down(4)
     h_pass(5)
     sum_over_cores()
-    down(4)
     down(5)
     h_pass(6)
     down(2)
@@ -570,35 +591,16 @@
     for a in range(1, ys):
         arrived(rs2_recv.at[a - 1], r2_send.at[a - 1], r2_recv.at[a - 1], over_y(a))
         total += rs2_recv[a - 1].astype(F32)
-    ret[...] = total.astype(BF16)
-    ret_store = pltpu.make_async_copy(ret, ret_out, out_sem.at[0])
-    ret_store.start()
+    ret_out[...] = total.astype(BF16)
     for k in range(split, ep):
         arrived(rbuf.at[block(k)], b_send.at[k], b_recv.at[k], pair(k))
-    exp[...] = (close + weighed(block(split, ep - split))).astype(BF16)
-    exp_store = pltpu.make_async_copy(exp, exp_out, out_sem.at[1])
-    exp_store.start()
+    exp_out[...] = (close + weighed(block(split, ep - split))).astype(BF16)
     for copy in sent[early:]:
         copy.wait_send()
-    ret_store.wait()
-    exp_store.wait()
 
     @pl.when(bit(last) == 0)
     def _():
         state_copy(last).wait_send()
-
-
-def hand_on(ret_in, exp_in, ret_out, exp_out, ret, exp, in_sem, out_sem):
-    ways = ((ret_in, ret, ret_out), (exp_in, exp, exp_out))
-    taken = [pltpu.make_async_copy(a, b, in_sem.at[i]) for i, (a, b, _) in enumerate(ways)]
-    given = [pltpu.make_async_copy(b, d, out_sem.at[i]) for i, (_, b, d) in enumerate(ways)]
-    for copy in taken:
-        copy.start()
-    for i in range(2):
-        taken[i].wait()
-        given[i].start()
-    for copy in given:
-        copy.wait()
 
 
 def body(
@@ -627,6 +629,7 @@
     slots = ep * cap
     rb = block_len // tp
     hbm = pl.BlockSpec(memory_space=pl.ANY)
+    vmem = pl.BlockSpec(memory_space=pltpu.VMEM)
     dma = pltpu.SemaphoreType.DMA
     given = [
         route_ids.T, token_rows, token_gain[None, :], expert_gate[0], expert_up[0],
@@ -637,12 +640,9 @@
     nm = len(GROUPS)
     outs = pl.pallas_call(
         functools.partial(kernel, size),
-        out_shape=(
-            jax.ShapeDtypeStruct((rb, model), BF16),
-            jax.ShapeDtypeStruct((tokens, cw), BF16),
-        ),
+        out_shape=(pltpu.VMEM((rb, model), BF16), pltpu.VMEM((tokens, cw), BF16)),
         in_specs=[hbm] * len(given),
-        out_specs=(hbm, hbm),
+        out_specs=(vmem, vmem),
         scratch_shapes=[
             (pltpu.SMEM if a is decay_rate else pltpu.VMEM)(a.shape, a.dtype) for a in given]
         + [
@@ -673,7 +673,7 @@
             pltpu.VMEM((ys, rb, model), BF16),
             pltpu.VMEM((max(ys - 1, 1), rb, model), BF16),
             pltpu.VMEM((max(ys - 1, 1), rb, model), BF16),
-            dma((len(given),)),
+            dma((len(given) + 2,)),
             dma((1,)), dma((1,)), dma((pieces,)), dma((pieces,)),
             dma((ys, pieces)), dma((ys, pieces)),
             dma((ep, pieces)), dma((ep, pieces)),
@@ -682,21 +682,12 @@
             dma((ep,)), dma((ep,)),
             dma((rounds,)), dma((rounds,)),
             dma((ys,)), dma((ys,)), dma((ys,)), dma((ys,)),
-            pltpu.VMEM((rb, model), BF16),
-            pltpu.VMEM((tokens, cw), BF16),
-            dma((2,)),
         ],
         compiler_params=pltpu.CompilerParams(
-            collective_id=0, has_side_effects=True, vmem_limit_bytes=60 * 2**20
+            collective_id=0, has_side_effects=True, vmem_limit_bytes=VMEM_LIMIT
         ),
     )(*given)
-    return pl.pallas_call(
-        hand_on,
-        out_shape=tuple(jax.ShapeDtypeStruct(a.shape, a.dtype) for a in outs),
-        in_specs=[hbm] * 2,
-        out_specs=(hbm, hbm),
-        scratch_shapes=[pltpu.VMEM(a.shape, a.dtype) for a in outs] + [dma((2,)), dma((2,))],
-    )(*outs)
+    return outs
 
 
 def solution(mesh):

time: 69.9 us -> 67.5 us (0.966)
  Pallas kernels: 68.9 us -> 65 us
  local copies, waits for them, and re-layouts: 0 us -> 1.47 us
    pallas_call x2 -> x1, Pallas kernels: 68.9 us -> 65 us  [body(): pl.pallas_call(functools.partial(kernel, size), out_shape=(pltpu.VMEM((rb...]
    unnamed x0 -> x2, local copies, waits for them, and re-layouts: none -> 1.47 us
where the time goes in v3:
time: 67.5 us; the launch traced here: 67.1 us
  Pallas kernels  65 us (96%)
  local copies, waits for them, and re-layouts  1.47 us (2%)
    pallas_call x1, Pallas kernels, body(): pl.pallas_call(functools.partial(kernel, size), out_shape=(pltpu.VMEM((rb...  65 us
    unnamed x2, local copies, waits for them, and re-layouts  1.47 us

profile of v3, /device:TPU:0, one launch (start us, length us, event | category | flops | bytes accessed | tf_op | source)
XLA Modules:
  0.0 67.1 jit_solution(787762186695999895)
XLA Ops:
  0.6 65.0 %shard_map.167 = (bf16[128,2048]{1,0:T(8,128)(2,1)S(1)}, bf16[192,512]{1,0:T(8,128)(2,1)S(1)}) custom-call(s32[2,192]{1,0:T(2,128)} %bitcast.11, bf16[192,2048]{1,0:T(8,128)(2,1)} %tok_h.1, f32[1,2048]{1,0:T(1,128)} %bitcast.10, bf16[2048,1024]{1,0:T(8,128)(2,1)} %bitcast.7, bf16[2048,1024]{1,0:T(8,128)(2,1)} %bitcast.8, bf16[512,512]{1,0:T(8,128)(2,1)} %query_h.1, ...), custom_call_target="tpu_custom_call" | custom-call | tf_op jit(solution)/shard_map/pallas_call | solution.py:641
  65.6 0.8 %copy.20 = bf16[128,2048]{1,0:T(8,128)(2,1)} copy(bf16[128,2048]{1,0:T(8,128)(2,1)S(1)} %get-tuple-element.2) | data formatting | bytes 1048576
  66.4 0.7 %copy.21 = bf16[192,512]{1,0:T(8,128)(2,1)} copy(bf16[192,512]{1,0:T(8,128)(2,1)S(1)} %get-tuple-element.3) | data formatting | bytes 393216

commit v4 on v3

--- a/solution.py
+++ b/solution.py
@@ -513,9 +513,9 @@
     for i in range(pieces):
         raw_push(i)
     up_mine(1)
-    x_relay(2)
     up_rest(1)
     up_send(1)
+    x_relay(2)
     h_pass(0)
     head_local(0, heads)
     raw_relay(0)
@@ -543,8 +543,8 @@
     up_send(4)
     x_relay(5)
     x_relay(6)
-    down(1)
-    up(5)
+    up_mine(5)
+    up_rest(5)
     up_send(5)
     h_pass(3)
     for r in range(3, rounds):
@@ -556,20 +556,21 @@
     loads["hgain"].wait()
     loads["ow"].wait()
     finish(0, heads)
+    h_pass(4)
     up(6)
     up_send(6)
-    h_pass(4)
     project()
+    down(4)
+    h_pass(5)
     up(7)
     up_send(7)
     early = len(sent)
-    down(4)
-    h_pass(5)
     sum_over_cores()
     down(5)
     h_pass(6)
+    down(1)
+    down(6)
     down(2)
-    down(6)
     down(3)
     loads["rweights"].wait()
     combine_weights()
@@ -592,11 +593,11 @@
         arrived(rs2_recv.at[a - 1], r2_send.at[a - 1], r2_recv.at[a - 1], over_y(a))
         total += rs2_recv[a - 1].astype(F32)
     ret_out[...] = total.astype(BF16)
+    for copy in sent[early:]:
+        copy.wait_send()
     for k in range(split, ep):
         arrived(rbuf.at[block(k)], b_send.at[k], b_recv.at[k], pair(k))
     exp_out[...] = (close + weighed(block(split, ep - split))).astype(BF16)
-    for copy in sent[early:]:
-        copy.wait_send()
 
     @pl.when(bit(last) == 0)
     def _():

time: 67.5 us -> 67.3 us (level)
  no operation moved by 1% of the time
where the time goes in v4:
time: 67.3 us; the launch traced here: 67.1 us
  Pallas kernels  65 us (97%)
  local copies, waits for them, and re-layouts  1.47 us (2%)
    pallas_call x1, Pallas kernels, body(): pl.pallas_call(functools.partial(kernel, size), out_shape=(pltpu.VMEM((rb...  65 us
    unnamed x2, local copies, waits for them, and re-layouts  1.47 us

profile of v4, /device:TPU:0, one launch (start us, length us, event | category | flops | bytes accessed | tf_op | source)
XLA Modules:
  0.0 67.1 jit_solution(14024536599699244851)
XLA Ops:
  0.6 65.0 %shard_map.167 = (bf16[128,2048]{1,0:T(8,128)(2,1)S(1)}, bf16[192,512]{1,0:T(8,128)(2,1)S(1)}) custom-call(s32[2,192]{1,0:T(2,128)} %bitcast.11, bf16[192,2048]{1,0:T(8,128)(2,1)} %tok_h.1, f32[1,2048]{1,0:T(1,128)} %bitcast.10, bf16[2048,1024]{1,0:T(8,128)(2,1)} %bitcast.7, bf16[2048,1024]{1,0:T(8,128)(2,1)} %bitcast.8, bf16[512,512]{1,0:T(8,128)(2,1)} %query_h.1, ...), custom_call_target="tpu_custom_call" | custom-call | tf_op jit(solution)/shard_map/pallas_call | solution.py:642
  65.7 0.8 %copy.20 = bf16[128,2048]{1,0:T(8,128)(2,1)} copy(bf16[128,2048]{1,0:T(8,128)(2,1)S(1)} %get-tuple-element.2) | data formatting | bytes 1048576
  66.5 0.7 %copy.21 = bf16[192,512]{1,0:T(8,128)(2,1)} copy(bf16[192,512]{1,0:T(8,128)(2,1)S(1)} %get-tuple-element.3) | data formatting | bytes 393216
